TPU v7x, 32 devices: a whole 2x2x4 slice. The times are simulated.
32 devices in a mesh: ep: 8 (over z, x), tp: 4 (over y, core).
Axes of the slice: x: 2, y: 2, z: 4, core: 2. Of those that a mesh axis runs over, the one named last changes fastest.
Arguments:
- queries: bfloat16 [4096, 2048], P('ep', 'tp'), may hold values from -5 to 5
- key_rows: bfloat16 [4096, 2048], P('ep', 'tp'), may hold values from -5 to 5
- values: bfloat16 [4096, 2048], P('ep', 'tp'), may hold values from -6 to 6
- forget_log: float32 [4096, 16], P(None, 'tp'), may hold values from -515 to 0, as said below
- out_weight: bfloat16 [2048, 4096], P(None, 'tp'), may hold values from -1 to 1
- expert_input: bfloat16 [1024, 4096], P(('ep', 'tp')), may hold values from -6 to 6
- norm_gain: float32 [4096], replicated, may hold values from 0.1 to 1.9
- route_ids: int32 [1024, 2], P('ep'), may hold values from 0 to 7, all different within a row; in each aligned block of 128 rows (0 to 127, 128 to 255, ...) at most 64 rows name the same one
- route_weights: float32 [1024, 2], P('ep'), may hold values from 0.2 to 1
- gate_weight: bfloat16 [8, 4096, 2048], P('ep', None, 'tp'), may hold values from -0.09375 to 0.09375
- up_weight: bfloat16 [8, 4096, 2048], P('ep', None, 'tp'), may hold values from -0.09375 to 0.09375
- down_weight: bfloat16 [8, 2048, 4096], P('ep', None, 'tp'), may hold values from -0.125 to 0.125
Outputs:
- mixer_out: bfloat16 [4096, 4096], P('ep', 'tp')
- expert_out: bfloat16 [1024, 4096], P('ep', 'tp')
Inputs may be any that keep to these rules, and one draw needn't show every extreme that they name: forget_log[t, h] is the sum of the log forget gates of head h at positions 0 to t of the one sequence; it never rises along positions. `route_ids`: each row names 2 different experts. In each aligned block of 128 rows (the rows of one index of ep) no expert is named by more than 64 rows, and some block reaches 64.
All inputs are finite; a program needn't handle non-finite values.
Results may differ from a plain program's by a relative error of at most 0.0071.
Values may be sent and summed in bfloat16 or wider, within the bound.
A program may use at most 64 MiB of HBM per device.

v0:
```python
import jax
import jax.numpy as jnp
from jax import lax
from jax.sharding import PartitionSpec as P

EPSILON = 1e-05


def slot_places(route_rows, experts, capacity):
    entries = route_rows.reshape(-1)
    matches = (entries[:, None] == jnp.arange(experts, dtype=jnp.int32)[None, :]).astype(jnp.int32)
    earlier = jnp.cumsum(matches, axis=0) - matches
    ranking = jnp.sum(earlier * matches, axis=1)
    return entries * capacity + ranking


def source_table(places, rows_count, chosen, total_slots):
    owners = jnp.arange(places.shape[0], dtype=jnp.int32) // chosen
    return jnp.full((total_slots,), rows_count, jnp.int32).at[places].set(owners)


def body(
    queries,
    key_rows,
    values,
    forget_log,
    out_weight,
    expert_input,
    norm_gain,
    route_ids,
    route_weights,
    gate_weight,
    up_weight,
    down_weight,
):
    row_count = queries.shape[0]
    heads_here = forget_log.shape[1]
    head_width = queries.shape[1] // heads_here
    own_start = lax.axis_index("ep") * row_count
    position_indices = own_start + jnp.arange(row_count, dtype=jnp.int32)
    query_heads = queries.reshape(row_count, heads_here, head_width)
    query_gate = lax.dynamic_slice_in_dim(forget_log, own_start, row_count, 0)
    score_scale = head_width ** (-0.5)

    def fold_shard(state_now, shard_item):
        first_row, key_shard, value_shard = shard_item

        def attend(state_in):
            row_max, row_total, weighted = state_in
            key_heads = key_shard.reshape(row_count, heads_here, head_width)
            value_heads = value_shard.reshape(row_count, heads_here, head_width)
            key_gate = lax.dynamic_slice_in_dim(forget_log, first_row, row_count, 0)
            scores = (
                jnp.einsum(
                    "qhd,khd->hqk", query_heads, key_heads, preferred_element_type=jnp.float32
                )
                * score_scale
            )
            scores = scores + query_gate.T[:, :, None] - key_gate.T[:, None, :]
            key_pos = first_row + jnp.arange(row_count, dtype=jnp.int32)
            scores = jnp.where(
                key_pos[None, None, :] <= position_indices[None, :, None], scores, -jnp.inf
            )
            newest = jnp.maximum(row_max, jnp.max(scores, axis=2))
            factor = jnp.exp(row_max - newest)
            weights_now = jnp.exp(scores - newest[:, :, None])
            row_total = row_total * factor + jnp.sum(weights_now, axis=2)
            weighted = weighted * factor[:, :, None] + jnp.einsum(
                "hqk,khd->hqd",
                weights_now.astype(jnp.bfloat16),
                value_heads,
                preferred_element_type=jnp.float32,
            )
            return (newest, row_total, weighted)

        return (
            lax.cond(first_row <= own_start, attend, lambda state_in: state_in, state_now),
            None,
        )

    initial = (
        jnp.full((heads_here, row_count), -jnp.inf, jnp.float32),
        jnp.zeros((heads_here, row_count), jnp.float32),
        jnp.zeros((heads_here, row_count, head_width), jnp.float32),
    )
    state_now = initial
    key_piece = lax.all_gather(key_rows, "ep", axis=0, tiled=True)
    value_piece = lax.all_gather(values, "ep", axis=0, tiled=True)
    shards = key_piece.shape[0] // row_count
    starts = row_count * jnp.arange(shards, dtype=jnp.int32)
    stacked = (
        starts,
        key_piece.reshape(shards, row_count, -1),
        value_piece.reshape(shards, row_count, -1),
    )
    state_now, _ = lax.scan(fold_shard, state_now, stacked)
    row_max, row_total, weighted = state_now
    attended = (
        (weighted / row_total[:, :, None])
        .transpose(1, 0, 2)
        .reshape(row_count, heads_here * head_width)
        .astype(jnp.bfloat16)
    )
    as_float = expert_input.astype(jnp.float32)
    center = jnp.mean(as_float, axis=1, keepdims=True)
    variance = jnp.mean(jnp.square(as_float - center), axis=1, keepdims=True)
    normed = ((as_float - center) * lax.rsqrt(variance + EPSILON) * norm_gain).astype(jnp.bfloat16)
    group_rows = lax.all_gather(normed, "tp", axis=0, tiled=True)
    block_rows = route_ids.shape[0]
    chosen = route_ids.shape[1]
    expert_local = gate_weight.shape[0]
    ep_count = lax.axis_size("ep")
    tp_count = lax.axis_size("tp")
    experts = expert_local * ep_count
    capacity = block_rows * chosen * 2 // experts
    places = slot_places(route_ids, experts, capacity)
    slot_table = source_table(places, block_rows, chosen, experts * capacity).reshape(
        ep_count, expert_local, capacity
    )
    share_size = capacity // tp_count
    part_table = lax.dynamic_slice_in_dim(
        slot_table, lax.axis_index("tp") * share_size, share_size, 2
    )
    outgoing = jnp.take(group_rows, part_table, axis=0, mode="fill", fill_value=0)
    arrived = lax.all_to_all(outgoing, "ep", split_axis=0, concat_axis=0, tiled=True)
    arrived_rows = lax.all_gather(arrived, "tp", axis=2, tiled=True)
    gate_part = jnp.einsum(
        "sxcd,xdf->sxcf", arrived_rows, gate_weight, preferred_element_type=jnp.float32
    )
    up_part = jnp.einsum(
        "sxcd,xdf->sxcf", arrived_rows, up_weight, preferred_element_type=jnp.float32
    )
    hidden = (jax.nn.silu(gate_part) * up_part).astype(jnp.bfloat16)
    slots_all = ep_count * expert_local * capacity
    flat_hidden = hidden.reshape(slots_all, hidden.shape[3])
    out_width = out_weight.shape[1]
    mixer_sum = jnp.dot(
        lax.all_gather(attended, "tp", axis=1, tiled=True),
        out_weight,
        preferred_element_type=jnp.float32,
    )
    part_rows = lax.all_gather(flat_hidden, "tp", axis=1, tiled=True)
    shaped = part_rows.reshape(ep_count, expert_local, capacity, part_rows.shape[1])
    product = jnp.einsum("sxcf,xfd->sxcd", shaped, down_weight, preferred_element_type=jnp.float32)
    expert_sum = product.reshape(slots_all, out_width)
    leaving = expert_sum.astype(jnp.bfloat16).reshape(ep_count, expert_local, capacity, out_width)
    returned = lax.all_to_all(leaving, "ep", split_axis=0, concat_axis=0, tiled=True)
    picked = jnp.take(returned.reshape(experts * capacity, out_width), places, axis=0).astype(
        jnp.float32
    )
    combined = jnp.sum(
        (picked * route_weights.reshape(-1)[:, None]).reshape(block_rows, chosen, out_width), axis=1
    )
    return (mixer_sum.astype(jnp.bfloat16), combined.astype(jnp.bfloat16))


def solution(mesh):
    placed = (
        P("ep", "tp"),
        P("ep", "tp"),
        P("ep", "tp"),
        P(None, "tp"),
        P(None, "tp"),
        P(("ep", "tp"), None),
        P(),
        P("ep", None),
        P("ep", None),
        P("ep", None, "tp"),
        P("ep", None, "tp"),
        P("ep", None, "tp"),
    )
    return jax.shard_map(
        body, mesh=mesh, in_specs=placed, out_specs=(P("ep", "tp"), P("ep", "tp")), check_vma=False
    )
```

profile of v0, /device:TPU:0, one launch (start us, length us, event | category | flops | bytes accessed | tf_op | source)
XLA Modules:
  0.0 390.9 jit_solution(14663094674887229282)
XLA Ops:
  7.2 1.1 convert_reduce_fusion
  8.3 1.2 fusion.49
  9.5 1.8 fusion.51
  11.4 0.8 copy.62
  12.5 0.7 broadcast_multiply_fusion
  14.4 1.4 scatter_custom_fusion
  16.0 14.9 %all-gather.13.cloned.1.call-done = bf16[128,4096]{1,0:T(8,128)(2,1)} async-done(((bf16[32,4096]{1,0:T(8,128)(2,1)}), bf16[128,4096]{1,0:T(8,128)(2,1)}) %all-gather.13.cloned.1.call-update) | async-done | bytes 1048592 | tf_op jit(solution)/shard_map/all_gather | solution.py:108
  30.9 3.6 gather_fusion
  34.6 31.5 %all_to_all.10 = bf16[8,1,16,4096]{3,2,1,0:T(8,128)(2,1)} all-to-all(bf16[8,1,16,4096]{3,2,1,0:T(8,128)(2,1)S(1)} %broadcast_select_fusion), channel_id=1, replica_groups=mesh['ep'=8,'tp'=4] {'ep'}, dimensions={0} | all-to-all | bytes 2097152 | tf_op jit(solution)/shard_map/all_to_all | solution.py:125
  67.6 31.4 %all-gather.15.cloned.1.call-done = bf16[8,1,64,4096]{3,2,0,1:T(8,128)(2,1)} async-done(((bf16[8,1,16,4096]{3,2,0,1:T(8,128)(2,1)}), bf16[8,1,64,4096]{3,2,0,1:T(8,128)(2,1)}) %all-gather.15.cloned.1.call-update) | async-done | bytes 4194320 | tf_op jit(solution)/shard_map/all_gather | solution.py:126
  98.9 5.9 %fusion.27 = f32[8,1,64,512]{3,2,0,1:T(8,128)S(1)} fusion(bf16[1,4096,512]{2,1,0:T(8,128)(2,1)} %param.25, bf16[8,1,64,4096]{3,2,0,1:T(8,128)(2,1)} %all-gather.15.cloned.1.call-done), kind=kOutput, calls=%fused_computation.33 | convolution fusion | flops 2147483648 | bytes 9437184 | tf_op jit(solution)/shard_map/sxcd,xdf->sxcf/dot_general | solution.py:127
  104.9 3.2 fusion.42
  108.9 0.7 constant_dynamic-slice_fusion.2
  109.6 64.3 %all-gather.7.cloned.1.call-done = bf16[4096,512]{1,0:T(8,128)(2,1)} async-done(((bf16[512,512]{1,0:T(8,128)(2,1)}), bf16[4096,512]{1,0:T(8,128)(2,1)}) %all-gather.7.cloned.1.call-update) | async-done | bytes 4194320 | tf_op jit(solution)/shard_map/all_gather | solution.py:87
  173.9 6.5 %copy.58 = bf16[8,512,512]{1,2,0:T(8,128)(2,1)} copy(bf16[8,512,512]{2,1,0:T(8,128)(2,1)} %bitcast.117) | data formatting | bytes 8388608
  180.3 66.9 %all-gather.9.cloned.1.call-done = bf16[4096,512]{1,0:T(8,128)(2,1)} async-done(((bf16[512,512]{1,0:T(8,128)(2,1)}), bf16[4096,512]{1,0:T(8,128)(2,1)}) %all-gather.9.cloned.1.call-update) | async-done | bytes 4194320 | tf_op jit(solution)/shard_map/all_gather | solution.py:88
  247.2 6.5 %copy.60 = bf16[8,512,512]{1,2,0:T(8,128)(2,1)} copy(bf16[8,512,512]{2,1,0:T(8,128)(2,1)} %bitcast.118) | data formatting | bytes 8388608
  253.8 20.4 %while.16 = (s32[]{:T(128)}, f32[4,512]{1,0:T(4,128)S(1)}, f32[4,512]{1,0:T(4,128)S(1)}, f32[4,512,128]{2,1,0:T(8,128)S(1)}, s32[8]{0:T(128)S(1)}, /*index=5*/s3...) while((s32[]{:T(128)}, f32[4,512]{1,0:T(4,128)S(1)}, ...), condition=%wide.region_5.6_spmd.clone.clone, body=%wide.region_0.5_spmd.clone.clone.sunk | while | flops 555488256 | bytes 19607904 | solution.py:96
  255.1 10.0 %conditional.4 = ((f32[4,512]{1,0:T(4,128)S(1)}, f32[4,512]{1,0:T(4,128)S(1)}, f32[4,512,128]{2,1,0:T(8,128)S(1)})) conditional(s32[]{:T(128)} %convert_element_type.100, (f32[4,512]{1,0:T(4,128)S(1)}, f32[4,512]{1,0:T(4,128)S(1)}, f32[4,512,128]{2,1,0:T(8,128)S(1)}) %tuple.54, (s32[]{:T(128)}, s32[]{:T(128)}, bf16[8,512,512]{1,2,0:T(8,128)(2,1)}, ...), branch_computations={%region_1.1_spmd, %region_2.4_spmd} | conditional | flops 555488256 | bytes 19605586 | solution.py:77
  257.0 0.8 dynamic-slice_bitcast_fusion
  258.7 1.3 constant_dynamic-slice_fusion
  259.9 1.4 fusion.4
  261.4 1.4 fusion.3
  262.8 2.3 fusion.8
  274.5 0.9 divide_convert_fusion
  275.5 6.1 %fusion.24 = bf16[8,1,64,1024]{3,2,1,0:T(8,128)(2,1)} fusion(bf16[8,64,2048]{2,1,0:T(8,128)(2,1)} %bitcast.129, bf16[1,2048,1024]{2,1,0:T(8,128)(2,1)} %param.27), kind=kOutput, calls=%fused_computation.32 | convolution fusion | flops 2148007936 | bytes 7340032 | tf_op jit(solution)/shard_map/sxcf,xfd->sxcd/dot_general | solution.py:144
  281.7 72.9 %all-to-all-start.1 = ((bf16[8,1,64,1024]{3,2,1,0:T(8,128)(2,1)}), bf16[8,1,64,1024]{3,2,1,0:T(8,128)(2,1)S(1)}, u32[]{:S(2)}, u32[]{:S(2)}) async-start(bf16[8,1,64,1024]{3,2,1,0:T(8,128)(2,1)} %fusion.24), calls=%async_computation.1 | async-start | bytes 2097152 | tf_op jit(solution)/shard_map/all_to_all | solution.py:147
  355.1 11.4 %all-gather.11.cloned.1.call-done = bf16[512,2048]{0,1:T(8,128)(2,1)} async-done(((bf16[512,512]{0,1:T(8,128)(2,1)}), bf16[512,2048]{0,1:T(8,128)(2,1)}) %all-gather.11.cloned.1.call-update) | async-done | bytes 2097168 | tf_op jit(solution)/shard_map/all_gather | solution.py:138
  366.5 6.1 %convolution_convert_fusion = bf16[512,1024]{1,0:T(8,128)(2,1)} fusion(bf16[512,2048]{0,1:T(8,128)(2,1)} %all-gather.11.cloned.1.call-done, bf16[2048,1024]{1,0:T(8,128)(2,1)} %param.20), kind=kOutput, calls=%fused_computation.31 | convolution fusion | flops 2148007936 | bytes 7340032 | tf_op jit(solution)/shard_map/dot_general | solution.py:137
  372.7 7.7 %all-to-all-done.1 = bf16[8,1,64,1024]{3,2,1,0:T(8,128)(2,1)S(1)} async-done(((bf16[8,1,64,1024]{3,2,1,0:T(8,128)(2,1)}), bf16[8,1,64,1024]{3,2,1,0:T(8,128)(2,1)S(1)}, u32[]{:S(2)}, u32[]{:S(2)}) %all-to-all-start.1) | async-done | bytes 1048608 | tf_op jit(solution)/shard_map/all_to_all | solution.py:147
  380.3 1.2 gather_fusion.1
  381.7 2.3 multiply_reduce_fusion
  (84 shorter events, 11.1 us)
Async XLA Ops:
  7.2 23.8 %all-gather.13.cloned.1.call-start = ((), (), s32[]{:S(2)}) async-start(), calls=%async_computation.5 | async-start | bytes 1310720 | tf_op jit(solution)/shard_map/all_gather | solution.py:108
  11.3 87.6 %all-gather.15.cloned.1.call-start = ((), (), s32[]{:S(2)}) async-start(), calls=%async_computation.6 | async-start | bytes 5242880 | tf_op jit(solution)/shard_map/all_gather | solution.py:126
  66.2 107.7 %all-gather.7.cloned.1.call-start = ((), (), s32[]{:S(2)}) async-start(), calls=%async_computation.2 | async-start | bytes 4718592 | tf_op jit(solution)/shard_map/all_gather | solution.py:87
  66.9 180.3 %all-gather.9.cloned.1.call-start = ((), (), s32[]{:S(2)}) async-start(), calls=%async_computation.3 | async-start | bytes 4718592 | tf_op jit(solution)/shard_map/all_gather | solution.py:88
  67.5 208.0 %all-gather.17.cloned.1.call-start = ((), (), s32[]{:S(2)}) async-start(), calls=%async_computation.7 | async-start | bytes 2621440 | tf_op jit(solution)/shard_map/all_gather | solution.py:142
  98.9 5.9 %copy-start.3 = (bf16[1,4096,512]{2,1,0:T(8,128)(2,1)S(1)}, bf16[1,4096,512]{2,1,0:T(8,128)(2,1)}, u32[]{:S(2)}) copy-start(bf16[1,4096,512]{2,1,0:T(8,128)(2,1)} %param.26) | copy-start | bytes 12582916
  98.9 5.9 %copy-start.4 = (bf16[8,1,64,4096]{3,2,0,1:T(8,128)(2,1)S(1)}, bf16[8,1,64,4096]{3,2,0,1:T(8,128)(2,1)}, u32[]{:S(2)}) copy-start(bf16[8,1,64,4096]{3,2,0,1:T(8,128)(2,1)} %all-gather.15.cloned.1.call-done) | copy-start | bytes 12582916
  104.9 3.5 copy-start
  108.1 258.4 %all-gather.11.cloned.1.call-start = ((), (), s32[]{:S(2)}) async-start(), calls=%async_computation.4 | async-start | bytes 2621440 | tf_op jit(solution)/shard_map/all_gather | solution.py:138
  275.5 79.3 %copy-start.1 = (s32[128,2]{0,1:T(2,128)S(1)}, s32[128,2]{0,1:T(2,128)}, u32[]{:S(2)}) copy-start(s32[128,2]{0,1:T(2,128)} %param.23) | copy-start | bytes 3076
  275.5 79.5 %copy-start.2 = (f32[128,2]{0,1:T(2,128)S(1)}, f32[128,2]{0,1:T(2,128)}, u32[]{:S(2)}) copy-start(f32[128,2]{0,1:T(2,128)} %param.24) | copy-start | bytes 3076
  281.7 98.6 %all-to-all-start.1 = ((bf16[8,1,64,1024]{3,2,1,0:T(8,128)(2,1)}), bf16[8,1,64,1024]{3,2,1,0:T(8,128)(2,1)S(1)}, u32[]{:S(2)}, u32[]{:S(2)}) async-start(bf16[8,1,64,1024]{3,2,1,0:T(8,128)(2,1)} %fusion.24), calls=%async_computation.1 | async-start | bytes 2097152 | tf_op jit(solution)/shard_map/all_to_all | solution.py:147
Sparse Core Ops, SparseCore 0:
  11.5 19.4 all-gather.12
  66.3 32.5 all-gather.14
  101.1 72.7 all-gather.6
  175.9 71.3 all-gather.8
  248.6 21.0 all-gather.16
  275.6 90.8 all-gather.10
where the time goes:
time: 392 us; the launch traced here: 391 us
  waiting for transfers between devices  198 us (51%)
  starting transfers between devices  73.3 us (19%)
  blocking collectives  31.5 us (8%)
  local copies, waits for them, and re-layouts  30 us (8%)
  matrix products  25.1 us (6%)
  between operations  14.3 us (4%)
  other arithmetic  11.3 us (3%)
  loops' own time  7.47 us (2%)
    all_to_all x1, starting transfers between devices, body(): lax.all_to_all(leaving, 'ep', split_axis=0, concat_axis=0, tiled=True)  72.9 us
    all_gather x1, waiting for transfers between devices, body(): value_piece = lax.all_gather(values, 'ep', axis=0, tiled=True)  66.9 us
    all_gather x1, waiting for transfers between devices, body(): key_piece = lax.all_gather(key_rows, 'ep', axis=0, tiled=True)  64.3 us
    all_to_all x1, blocking collectives, body(): lax.all_to_all(outgoing, 'ep', split_axis=0, concat_axis=0, tiled=True)  31.5 us
    all_gather x1, waiting for transfers between devices, body(): arrived_rows = lax.all_gather(arrived, 'tp', axis=2, tiled=True)  31.4 us
    all_gather x1, waiting for transfers between devices, body(): group_rows = lax.all_gather(normed, 'tp', axis=0, tiled=True)  14.9 us
    unnamed x16, local copies, waits for them, and re-layouts  14.4 us
    all_gather x1, waiting for transfers between devices, body(): lax.all_gather(attended, 'tp', axis=1, tiled=True)  11.4 us
  transfers between devices with their start and end apart: 7, of which 6 were waited for; matrix products, arithmetic and copies ran while one was open for 14% of the time, Pallas kernels for 0%

commit v1 on v0

v1 whole, which is shorter than its diff:
```python
import functools
import math

import jax
import jax.numpy as jnp
from jax import lax
from jax.experimental import pallas as pl
from jax.experimental.pallas import tpu as pltpu
from jax.sharding import PartitionSpec as P

EPSILON = 1e-05
LOG2E = math.log2(math.e)


def attention_kernel(
    n, heads, gate_row, gate_col, q_ref, k_ref, v_ref, out_ref,
    k_buf, v_buf, q_buf, o_buf,
    recv_k, recv_v, recv_q, recv_o, send_k, send_v, send_q, send_o, pass_k, pass_v,
):
    members = n // heads
    rows = k_ref.shape[0]
    width = k_ref.shape[1] // heads
    chunk = rows // members
    me = lax.axis_index("ep")
    my_member = me % members
    my_head = me // members

    barrier = pltpu.get_barrier_semaphore()

    @pl.loop(1, n)
    def _(step):
        pl.semaphore_signal(barrier, inc=1, device_id={"ep": (me + step) % n})

    pl.semaphore_wait(barrier, n - 1)

    def k_copy(target, head):
        cols = pl.ds(pl.multiple_of(head * width, width), width)
        return pltpu.make_async_remote_copy(
            src_ref=k_ref.at[:, cols], dst_ref=k_buf.at[me], send_sem=send_k.at[head],
            recv_sem=recv_k.at[me], device_id={"ep": target},
        )

    def v_copy(target, head):
        cols = pl.ds(pl.multiple_of(head * width, width), width)
        return pltpu.make_async_remote_copy(
            src_ref=v_ref.at[:, cols], dst_ref=v_buf.at[me], send_sem=send_v.at[head],
            recv_sem=recv_v.at[me], device_id={"ep": target},
        )

    def q_copy(target):
        cols = pl.ds(pl.multiple_of((target // members) * width, width), width)
        part = pl.ds(pl.multiple_of((target % members) * chunk, chunk), chunk)
        return pltpu.make_async_remote_copy(
            src_ref=q_ref.at[part, cols], dst_ref=q_buf.at[me], send_sem=send_q.at[target],
            recv_sem=recv_q.at[me], device_id={"ep": target},
        )

    def pass_copies(source, target):
        return (
            pltpu.make_async_remote_copy(
                src_ref=k_buf.at[source], dst_ref=k_buf.at[source],
                send_sem=pass_k.at[source, target % members],
                recv_sem=recv_k.at[source], device_id={"ep": target},
            ),
            pltpu.make_async_remote_copy(
                src_ref=v_buf.at[source], dst_ref=v_buf.at[source],
                send_sem=pass_v.at[source, target % members],
                recv_sem=recv_v.at[source], device_id={"ep": target},
            ),
        )

    def back_copy(source):
        cols = pl.ds(pl.multiple_of(my_head * width, width), width)
        part = pl.ds(pl.multiple_of(my_member * chunk, chunk), chunk)
        return pltpu.make_async_remote_copy(
            src_ref=o_buf.at[source], dst_ref=out_ref.at[part, cols], send_sem=send_o.at[source],
            recv_sem=recv_o.at[me], device_id={"ep": source},
        )

    own_cols = pl.ds(pl.multiple_of(my_head * width, width), width)
    own_part = pl.ds(pl.multiple_of(my_member * chunk, chunk), chunk)
    pltpu.make_async_copy(k_ref.at[:, own_cols], k_buf.at[me], recv_k.at[me]).start()
    pltpu.make_async_copy(v_ref.at[:, own_cols], v_buf.at[me], recv_v.at[me]).start()
    pltpu.make_async_copy(q_ref.at[own_part, own_cols], q_buf.at[me], recv_q.at[me]).start()

    @pl.loop(1, heads)
    def _(step):
        head = (my_head + step) % heads
        k_copy(head * members + my_member, head).start()
        v_copy(head * members + my_member, head).start()

    @pl.loop(1, n)
    def _(step):
        q_copy((me + step) % n).start()

    def landed(source):
        pltpu.make_async_copy(k_buf.at[source], k_buf.at[source], recv_k.at[source]).wait()
        pltpu.make_async_copy(v_buf.at[source], v_buf.at[source], recv_v.at[source]).wait()

    @pl.loop(0, heads)
    def _(step):
        source = ((my_head + step) % heads) * members + my_member
        landed(source)

        @pl.loop(1, members)
        def _(other):
            for copy in pass_copies(source, my_head * members + (my_member + other) % members):
                copy.start()

    column = lax.broadcasted_iota(jnp.int32, (chunk, rows), 1)
    line = lax.broadcasted_iota(jnp.int32, (chunk, rows), 0) + my_member * chunk
    causal = column <= line
    factor = LOG2E * width ** (-0.5)

    @pl.loop(0, n)
    def _(i):
        pltpu.make_async_copy(q_buf.at[i], q_buf.at[i], recv_q.at[i]).wait()

        @pl.when(i % members != my_member)
        def _():
            landed(i)

        query = q_buf[i]
        line_gate = gate_col[i]

        def scores_of(j):
            raw = lax.dot_general(
                query, k_buf[j], (((1,), (1,)), ((), ())), preferred_element_type=jnp.float32
            )
            return raw * factor + (line_gate - gate_row[j])

        def weigh(weights, j):
            return jnp.dot(
                weights.astype(jnp.bfloat16), v_buf[j], preferred_element_type=jnp.float32
            )

        scores = jnp.where(causal, scores_of(i), -jnp.inf)
        top = jnp.max(scores, axis=1, keepdims=True)
        weights = jnp.exp2(scores - top)
        total = jnp.sum(weights, axis=1, keepdims=True)
        held = weigh(weights, i)

        def fold(j, state):
            top, total, held = state
            scores = scores_of(j)
            newest = jnp.maximum(top, jnp.max(scores, axis=1, keepdims=True))
            shrink = jnp.exp2(top - newest)
            weights = jnp.exp2(scores - newest)
            total = total * shrink + jnp.sum(weights, axis=1, keepdims=True)
            held = held * shrink + weigh(weights, j)
            return newest, total, held

        top, total, held = lax.fori_loop(0, i, fold, (top, total, held))
        o_buf[i] = (held / total).astype(o_buf.dtype)

        @pl.when(i != me)
        def _():
            back_copy(i).start()

    own = pltpu.make_async_copy(o_buf.at[me], out_ref.at[own_part, own_cols], recv_o.at[me])
    own.start()

    @pl.loop(1, heads)
    def _(step):
        head = (my_head + step) % heads
        k_copy(head * members + my_member, head).wait_send()
        v_copy(head * members + my_member, head).wait_send()

    @pl.loop(1, n)
    def _(step):
        q_copy((me + step) % n).wait_send()
        back_copy((me + step) % n).wait_send()

    @pl.loop(0, heads)
    def _(step):
        source = step * members + my_member

        @pl.loop(1, members)
        def _(other):
            for copy in pass_copies(source, my_head * members + (my_member + other) % members):
                copy.wait_send()

    @pl.loop(0, n)
    def _(i):
        cols = pl.ds(pl.multiple_of((i // members) * width, width), width)
        part = pl.ds(pl.multiple_of((i % members) * chunk, chunk), chunk)
        spot = out_ref.at[part, cols]
        pltpu.make_async_copy(spot, spot, recv_o.at[i]).wait()


def attention(queries, key_rows, values, forget_log):
    n = lax.axis_size("ep")
    rows, heads = queries.shape[0], forget_log.shape[1]
    width = queries.shape[1] // heads
    members = n // heads
    chunk = rows // members
    me = lax.axis_index("ep")
    gates = lax.dynamic_slice_in_dim(forget_log.T * LOG2E, me // members, 1, 0)
    gate_row = gates.reshape(n, 1, rows)
    gate_col = lax.dynamic_slice_in_dim(
        gates.reshape(n, members, chunk), me % members, 1, 1
    ).reshape(n, chunk, 1)
    vmem = pl.BlockSpec(memory_space=pltpu.VMEM)
    dma = pltpu.SemaphoreType.DMA
    blocks = n * (n + 1) // 2
    return pl.pallas_call(
        functools.partial(attention_kernel, n, heads),
        out_shape=jax.ShapeDtypeStruct((rows, heads * width), jnp.bfloat16),
        in_specs=[vmem] * 5,
        out_specs=vmem,
        scratch_shapes=[
            pltpu.VMEM((n, rows, width), jnp.bfloat16),
            pltpu.VMEM((n, rows, width), jnp.bfloat16),
            pltpu.VMEM((n, chunk, width), jnp.bfloat16),
            pltpu.VMEM((n, chunk, width), jnp.bfloat16),
            dma((n,)), dma((n,)), dma((n,)), dma((n,)),
            dma((heads,)), dma((heads,)), dma((n,)), dma((n,)),
            dma((n, members)), dma((n, members)),
        ],
        compiler_params=pltpu.CompilerParams(
            collective_id=0, has_side_effects=True, vmem_limit_bytes=40 * 1024 * 1024
        ),
        cost_estimate=pl.CostEstimate(
            flops=40 * blocks * chunk * rows * width, bytes_accessed=8 * rows * heads * width,
            transcendentals=blocks * chunk * rows,
        ),
    )(gate_row, gate_col, queries, key_rows, values)


def slot_places(route_rows, experts, capacity):
    entries = route_rows.reshape(-1)
    matches = (entries[:, None] == jnp.arange(experts, dtype=jnp.int32)[None, :]).astype(jnp.int32)
    earlier = jnp.cumsum(matches, axis=0) - matches
    ranking = jnp.sum(earlier * matches, axis=1)
    return entries * capacity + ranking


def source_table(places, rows_count, chosen, total_slots):
    owners = jnp.arange(places.shape[0], dtype=jnp.int32) // chosen
    return jnp.full((total_slots,), rows_count, jnp.int32).at[places].set(owners)


def body(
    queries,
    key_rows,
    values,
    forget_log,
    out_weight,
    expert_input,
    norm_gain,
    route_ids,
    route_weights,
    gate_weight,
    up_weight,
    down_weight,
):
    as_float = expert_input.astype(jnp.float32)
    center = jnp.mean(as_float, axis=1, keepdims=True)
    variance = jnp.mean(jnp.square(as_float - center), axis=1, keepdims=True)
    normed = ((as_float - center) * lax.rsqrt(variance + EPSILON) * norm_gain).astype(jnp.bfloat16)
    group_rows = lax.all_gather(normed, "tp", axis=0, tiled=True)
    block_rows = route_ids.shape[0]
    chosen = route_ids.shape[1]
    expert_local = gate_weight.shape[0]
    ep_count = lax.axis_size("ep")
    tp_count = lax.axis_size("tp")
    experts = expert_local * ep_count
    capacity = block_rows * chosen * 2 // experts
    places = slot_places(route_ids, experts, capacity)
    slot_table = source_table(places, block_rows, chosen, experts * capacity).reshape(
        ep_count, expert_local, capacity
    )
    share_size = capacity // tp_count
    part_table = lax.dynamic_slice_in_dim(
        slot_table, lax.axis_index("tp") * share_size, share_size, 2
    )
    outgoing = jnp.take(group_rows, part_table, axis=0, mode="fill", fill_value=0)
    arrived = lax.all_to_all(outgoing, "ep", split_axis=0, concat_axis=0, tiled=True)
    arrived, queries = lax.optimization_barrier((arrived, queries))
    attended = attention(queries, key_rows, values, forget_log)
    arrived_rows = lax.all_gather(arrived, "tp", axis=2, tiled=True)
    arrived_rows, attended = lax.optimization_barrier((arrived_rows, attended))
    gate_part = jnp.einsum(
        "sxcd,xdf->sxcf", arrived_rows, gate_weight, preferred_element_type=jnp.float32
    )
    up_part = jnp.einsum(
        "sxcd,xdf->sxcf", arrived_rows, up_weight, preferred_element_type=jnp.float32
    )
    hidden = (jax.nn.silu(gate_part) * up_part).astype(jnp.bfloat16)
    slots_all = ep_count * expert_local * capacity
    flat_hidden = hidden.reshape(slots_all, hidden.shape[3])
    out_width = out_weight.shape[1]
    mixer_sum = jnp.dot(
        lax.all_gather(attended, "tp", axis=1, tiled=True),
        out_weight,
        preferred_element_type=jnp.float32,
    )
    part_rows = lax.all_gather(flat_hidden, "tp", axis=1, tiled=True)
    shaped = part_rows.reshape(ep_count, expert_local, capacity, part_rows.shape[1])
    product = jnp.einsum("sxcf,xfd->sxcd", shaped, down_weight, preferred_element_type=jnp.float32)
    expert_sum = product.reshape(slots_all, out_width)
    leaving = expert_sum.astype(jnp.bfloat16).reshape(ep_count, expert_local, capacity, out_width)
    returned = lax.all_to_all(leaving, "ep", split_axis=0, concat_axis=0, tiled=True)
    picked = jnp.take(returned.reshape(experts * capacity, out_width), places, axis=0).astype(
        jnp.float32
    )
    combined = jnp.sum(
        (picked * route_weights.reshape(-1)[:, None]).reshape(block_rows, chosen, out_width), axis=1
    )
    return (mixer_sum.astype(jnp.bfloat16), combined.astype(jnp.bfloat16))


def solution(mesh):
    placed = (
        P("ep", "tp"),
        P("ep", "tp"),
        P("ep", "tp"),
        P(None, "tp"),
        P(None, "tp"),
        P(("ep", "tp"), None),
        P(),
        P("ep", None),
        P("ep", None),
        P("ep", None, "tp"),
        P("ep", None, "tp"),
        P("ep", None, "tp"),
    )
    return jax.shard_map(
        body, mesh=mesh, in_specs=placed, out_specs=(P("ep", "tp"), P("ep", "tp")), check_vma=False
    )
```

time: 392 us -> 225 us (0.57)
  waiting for transfers between devices: 198 us -> 73.2 us
  starting transfers between devices: 73.3 us -> 5.67 us
  Pallas kernels: 0 us -> 59.9 us
  local copies, waits for them, and re-layouts: 30 us -> 9.39 us
  loops' own time: 7.47 us -> 0 us
    all_gather x2 -> x0, waiting for transfers between devices: 131 us -> none  [the longest x1 66.9 us: body(): value_piece = lax.all_gather(values, 'ep', axis=0, tiled=True)]
    all_to_all x1, starting transfers between devices: 72.9 us -> 5.51 us  [body(): lax.all_to_all(leaving, 'ep', split_axis=0, concat_axis=0, tiled=True)]
    pallas_call x0 -> x1, Pallas kernels: none -> 59.9 us  [attention(): pl.pallas_call(functools.partial(attention_kernel, n, heads), out_shape=j...]
    all_gather x1, waiting for transfers between devices: 0.02 us -> 38.2 us  [body(): part_rows = lax.all_gather(flat_hidden, 'tp', axis=1, tiled=True)]
    all_gather x1, waiting for transfers between devices: 31.4 us -> 0.02 us  [body(): arrived_rows = lax.all_gather(arrived, 'tp', axis=2, tiled=True)]
    unnamed x16, local copies, waits for them, and re-layouts: 14.4 us -> 0.94 us
    another operation x9 -> x0, loops' own time: 7.47 us -> none  [the longest x1 5.38 us: body(): state_now, _ = lax.scan(fold_shard, state_now, stacked)]
    dynamic_slice x10 -> x1, local copies, waits for them, and re-layouts: 6.85 us -> 0.03 us  [attention(): lax.dynamic_slice_in_dim(gates.reshape(n, members, chunk), me % members,...]
  transfers between devices with their start and end apart: 7 -> 5, of which waited for: 6 -> 4; matrix products, arithmetic and copies ran while one was open for 14% -> 9% of each run, Pallas kernels for 0% -> 27%
where the time goes in v1:
time: 225 us
  waiting for transfers between devices  73.2 us (33%)
  Pallas kernels  59.9 us (27%)
  blocking collectives  31.7 us (14%)
  matrix products  21.4 us (10%)
  between operations  14 us (6%)
  other arithmetic  9.68 us (4%)
  local copies, waits for them, and re-layouts  9.39 us (4%)
  starting transfers between devices  5.67 us (3%)
    pallas_call x1, Pallas kernels, attention(): pl.pallas_call(functools.partial(attention_kernel, n, heads), out_shape=j...  59.9 us
    all_gather x1, waiting for transfers between devices, body(): part_rows = lax.all_gather(flat_hidden, 'tp', axis=1, tiled=True)  38.2 us
    all_to_all x1, blocking collectives, body(): lax.all_to_all(outgoing, 'ep', split_axis=0, concat_axis=0, tiled=True)  31.7 us
    all_gather x1, waiting for transfers between devices, body(): group_rows = lax.all_gather(normed, 'tp', axis=0, tiled=True)  14.9 us
    all_gather x1, waiting for transfers between devices, body(): lax.all_gather(attended, 'tp', axis=1, tiled=True)  11.8 us
    all_to_all x1, waiting for transfers between devices, body(): lax.all_to_all(leaving, 'ep', split_axis=0, concat_axis=0, tiled=True)  7.69 us
    dot_general x1, matrix products, body(): jnp.einsum('sxcf,xfd->sxcd', shaped, down_weight, preferred_element_type=...  6.15 us
    dot_general x1, matrix products, body(): jnp.dot(lax.all_gather(attended, 'tp', axis=1, tiled=True), out_weight, p...  6.12 us
  transfers between devices with their start and end apart: 5, of which 4 were waited for; matrix products, arithmetic and copies ran while one was open for 9% of the time, Pallas kernels for 27%

profile of v1, /device:TPU:0, one launch (start us, length us, event | category | flops | bytes accessed | tf_op | source)
XLA Modules:
  0.0 224.9 jit_solution(197418644367039623)
XLA Ops:
  7.2 1.1 convert_reduce_fusion
  8.3 1.2 fusion.36
  9.5 1.8 fusion.38
  11.4 0.8 copy.29
  12.2 0.1 eq.31
  12.3 0.1 eq.27
  12.5 0.6 reduce-window.6
  13.1 0.2 slice_reduce_fusion
  13.3 0.7 broadcast_multiply_fusion
  14.1 0.1 mul.66
  14.4 1.4 scatter_custom_fusion
  16.0 14.9 %all-gather.5.cloned.1.call-done = bf16[128,4096]{1,0:T(8,128)(2,1)} async-done(((bf16[32,4096]{1,0:T(8,128)(2,1)}), bf16[128,4096]{1,0:T(8,128)(2,1)}) %all-gather.5.cloned.1.call-update) | async-done | bytes 1048592 | tf_op jit(solution)/shard_map/all_gather | solution.py:261
  30.9 3.6 %gather_fusion = bf16[128,4096]{1,0:T(8,128)(2,1)S(1)} fusion(bf16[128,4096]{1,0:T(8,128)(2,1)} %all-gather.5.cloned.1.call-done, s32[1024]{0:T(1024)S(1)} %pad_clamp_fusion.1), kind=kCustom, calls=%fused_computation | custom fusion | bytes 2097664 | tf_op jit(solution)/shard_map/jit(_take)/gather | solution.py:277
  34.5 0.1 broadcast_select_fusion.1
  34.7 31.7 %all_to_all.10 = bf16[8,1,16,4096]{3,2,1,0:T(8,128)(2,1)} all-to-all(bf16[8,1,16,4096]{3,2,1,0:T(8,128)(2,1)S(1)} %broadcast_select_fusion.1), channel_id=1, replica_groups=mesh['ep'=8,'tp'=4] {'ep'}, dimensions={0} | all-to-all | bytes 2097152 | tf_op jit(solution)/shard_map/all_to_all | solution.py:278
  66.4 0.5 broadcast.137
  67.0 1.5 fusion.44
  68.6 0.3 reshape.187.gate_col
  68.9 59.9 %shard_map.131 = bf16[512,512]{1,0:T(8,128)(2,1)} custom-call(f32[8,1,512]{2,1,0:T(1,128)S(1)} %bitcast.86, f32[8,256,1]{2,1,0:T(8,128)S(1)} %reshape.187.gate_col, bf16[512,512]{1,0:T(8,128)(2,1)S(1)} %copy-done, bf16[512,512]{1,0:T(8,128)(2,1)S(1)} %copy-done.1, bf16[512,512]{1,0:T(8,128)(2,1)S(1)} %copy-done.2), custom_call_target="tpu_custom_call" | custom-call | flops 24159191040 | bytes 2097152 | tf_op jit(solution)/shard_map/pallas_call | solution.py:206
  128.9 5.9 %fusion.14 = f32[8,1,64,512]{3,2,0,1:T(8,128)S(1)} fusion(bf16[1,4096,512]{2,1,0:T(8,128)(2,1)} %param.21, bf16[8,1,64,4096]{3,2,1,0:T(8,128)(2,1)} %all-gather.7.cloned.1.call-done), kind=kOutput, calls=%fused_computation.14 | convolution fusion | flops 2147483648 | bytes 9437184 | tf_op jit(solution)/shard_map/sxcd,xdf->sxcf/dot_general | solution.py:283
  134.8 3.2 %fusion.29 = bf16[8,1,64,512]{3,2,0,1:T(8,128)(2,1)} fusion(bf16[1,4096,512]{2,1,0:T(8,128)(2,1)S(1)} %copy-done.5, bf16[8,1,64,4096]{3,2,1,0:T(8,128)(2,1)S(1)} %copy-done.6, f32[8,1,64,512]{3,2,0,1:T(8,128)S(1)} %fusion.14), kind=kOutput, calls=%fused_computation.17 | convolution fusion | flops 2149056512 | bytes 9961472 | tf_op jit(solution)/shard_map/sxcd,xdf->sxcf/dot_general | solution.py:286
  138.1 0.5 all-gather.9.cloned.1.call-update
  138.7 38.2 %all-gather.11.cloned.1.call-done = bf16[512,2048]{1,0:T(8,128)(2,1)} async-done(((bf16[512,512]{1,0:T(8,128)(2,1)}), bf16[512,2048]{1,0:T(8,128)(2,1)}) %all-gather.11.cloned.1.call-update) | async-done | bytes 2097168 | tf_op jit(solution)/shard_map/all_gather | solution.py:298
  176.8 6.2 %fusion.11 = bf16[8,1,64,1024]{3,2,1,0:T(8,128)(2,1)} fusion(bf16[8,64,2048]{2,1,0:T(8,128)(2,1)} %bitcast.93, bf16[1,2048,1024]{2,1,0:T(8,128)(2,1)} %param.23), kind=kOutput, calls=%fused_computation.13 | convolution fusion | flops 2148007936 | bytes 7340032 | tf_op jit(solution)/shard_map/sxcf,xfd->sxcd/dot_general | solution.py:300
  183.0 5.5 %all-to-all-start.1 = ((bf16[8,1,64,1024]{3,2,1,0:T(8,128)(2,1)}), bf16[8,1,64,1024]{3,2,1,0:T(8,128)(2,1)S(1)}, u32[]{:S(2)}, u32[]{:S(2)}) async-start(bf16[8,1,64,1024]{3,2,1,0:T(8,128)(2,1)} %fusion.11), calls=%async_computation.1 | async-start | bytes 2097152 | tf_op jit(solution)/shard_map/all_to_all | solution.py:303
  188.7 0.1 copy.34
  189.0 11.8 %all-gather.9.cloned.1.call-done = bf16[512,2048]{1,0:T(8,128)(2,1)} async-done(((bf16[512,512]{1,0:T(8,128)(2,1)}), bf16[512,2048]{1,0:T(8,128)(2,1)}) %all-gather.9.cloned.1.call-update) | async-done | bytes 2097168 | tf_op jit(solution)/shard_map/all_gather | solution.py:294
  200.8 6.1 %convolution_convert_fusion = bf16[512,1024]{1,0:T(8,128)(2,1)} fusion(bf16[512,2048]{1,0:T(8,128)(2,1)} %all-gather.9.cloned.1.call-done, bf16[2048,1024]{1,0:T(8,128)(2,1)} %param.16), kind=kOutput, calls=%fused_computation.12 | convolution fusion | flops 2148007936 | bytes 7340032 | tf_op jit(solution)/shard_map/dot_general | solution.py:293
  207.0 7.7 %all-to-all-done.1 = bf16[8,1,64,1024]{3,2,1,0:T(8,128)(2,1)S(1)} async-done(((bf16[8,1,64,1024]{3,2,1,0:T(8,128)(2,1)}), bf16[8,1,64,1024]{3,2,1,0:T(8,128)(2,1)S(1)}, u32[]{:S(2)}, u32[]{:S(2)}) %all-to-all-start.1) | async-done | bytes 1048608 | tf_op jit(solution)/shard_map/all_to_all | solution.py:303
  214.6 1.2 gather_fusion.1
  215.8 0.2 gather.12
  216.0 2.3 %multiply_reduce_fusion = bf16[128,1024]{1,0:T(8,128)(2,1)} fusion(bf16[128,2,1024]{2,1,0:T(2,128)(2,1)S(1)} %gather.12, pred[128,2]{1,0:T(8,128)(4,1)S(1)} %copy.34, f32[128,2]{1,0:T(8,128)S(1)} %copy.36), kind=kLoop, calls=%fused_computation.18 | loop fusion | flops 917504 | bytes 787712 | tf_op jit(solution)/shard_map/reduce_sum | solution.py:307
  (42 shorter events, 1.2 us)
Async XLA Ops:
  7.2 23.8 %all-gather.5.cloned.1.call-start = ((), (), s32[]{:S(2)}) async-start(), calls=%async_computation.2 | async-start | bytes 1310720 | tf_op jit(solution)/shard_map/all_gather | solution.py:261
  11.3 117.5 %all-gather.7.cloned.1.call-start = ((), (), s32[]{:S(2)}) async-start(), calls=%async_computation.3 | async-start | bytes 5242880 | tf_op jit(solution)/shard_map/all_gather | solution.py:281
  34.5 34.4 %copy-start = (bf16[512,512]{1,0:T(8,128)(2,1)S(1)}, bf16[512,512]{1,0:T(8,128)(2,1)}, u32[]{:S(2)}) copy-start(bf16[512,512]{1,0:T(8,128)(2,1)} %q_ref) | copy-start | bytes 1572868
  34.5 34.4 %copy-start.1 = (bf16[512,512]{1,0:T(8,128)(2,1)S(1)}, bf16[512,512]{1,0:T(8,128)(2,1)}, u32[]{:S(2)}) copy-start(bf16[512,512]{1,0:T(8,128)(2,1)} %k_ref.1) | copy-start | bytes 1572868
  34.5 34.4 %copy-start.2 = (bf16[512,512]{1,0:T(8,128)(2,1)S(1)}, bf16[512,512]{1,0:T(8,128)(2,1)}, u32[]{:S(2)}) copy-start(bf16[512,512]{1,0:T(8,128)(2,1)} %v_ref.1) | copy-start | bytes 1572868
  66.4 110.5 %all-gather.11.cloned.1.call-start = ((), (), s32[]{:S(2)}) async-start(), calls=%async_computation.5 | async-start | bytes 2621440 | tf_op jit(solution)/shard_map/all_gather | solution.py:298
  128.9 6.0 %copy-start.5 = (bf16[1,4096,512]{2,1,0:T(8,128)(2,1)S(1)}, bf16[1,4096,512]{2,1,0:T(8,128)(2,1)}, u32[]{:S(2)}) copy-start(bf16[1,4096,512]{2,1,0:T(8,128)(2,1)} %param.22) | copy-start | bytes 12582916
  128.9 6.0 %copy-start.6 = (bf16[8,1,64,4096]{3,2,1,0:T(8,128)(2,1)S(1)}, bf16[8,1,64,4096]{3,2,1,0:T(8,128)(2,1)}, u32[]{:S(2)}) copy-start(bf16[8,1,64,4096]{3,2,1,0:T(8,128)(2,1)} %all-gather.7.cloned.1.call-done) | copy-start | bytes 12582916
  138.1 62.8 %all-gather.9.cloned.1.call-start = ((), (), s32[]{:S(2)}) async-start(), calls=%async_computation.4 | async-start | bytes 2621440 | tf_op jit(solution)/shard_map/all_gather | solution.py:294
  176.8 11.9 %copy-start.3 = (s32[128,2]{0,1:T(2,128)S(1)}, s32[128,2]{0,1:T(2,128)}, u32[]{:S(2)}) copy-start(s32[128,2]{0,1:T(2,128)} %param.19) | copy-start | bytes 3076
  176.8 12.0 %copy-start.4 = (f32[128,2]{0,1:T(2,128)S(1)}, f32[128,2]{0,1:T(2,128)}, u32[]{:S(2)}) copy-start(f32[128,2]{0,1:T(2,128)} %param.20) | copy-start | bytes 3076
  183.0 31.7 %all-to-all-start.1 = ((bf16[8,1,64,1024]{3,2,1,0:T(8,128)(2,1)}), bf16[8,1,64,1024]{3,2,1,0:T(8,128)(2,1)S(1)}, u32[]{:S(2)}, u32[]{:S(2)}) async-start(bf16[8,1,64,1024]{3,2,1,0:T(8,128)(2,1)} %fusion.11), calls=%async_computation.1 | async-start | bytes 2097152 | tf_op jit(solution)/shard_map/all_to_all | solution.py:303
Sparse Core Ops, SparseCore 0:
  11.5 19.4 all-gather.4
  66.5 32.5 all-gather.6
  138.2 38.5 all-gather.10
  178.2 22.5 all-gather.8

commit v2 on v1

--- a/solution.py
+++ b/solution.py
@@ -13,9 +13,11 @@
 
 
 def attention_kernel(
-    n, heads, gate_row, gate_col, q_ref, k_ref, v_ref, out_ref,
-    k_buf, v_buf, q_buf, o_buf,
+    n, tp, heads, gate_row, gate_col, q_ref, k_ref, v_ref, pick_ref, token_ref,
+    out_ref, routed_ref,
+    k_buf, v_buf, q_buf, o_buf, token_buf, leave_buf,
     recv_k, recv_v, recv_q, recv_o, send_k, send_v, send_q, send_o, pass_k, pass_v,
+    send_t, recv_t, send_a, recv_a, send_f, recv_f,
 ):
     members = n // heads
     rows = k_ref.shape[0]
@@ -24,6 +26,8 @@
     me = lax.axis_index("ep")
     my_member = me % members
     my_head = me // members
+    my_tp = lax.axis_index("tp")
+    tokens = token_ref.shape[0]
 
     barrier = pltpu.get_barrier_semaphore()
 
@@ -31,7 +35,11 @@
     def _(step):
         pl.semaphore_signal(barrier, inc=1, device_id={"ep": (me + step) % n})
 
-    pl.semaphore_wait(barrier, n - 1)
+    @pl.loop(1, tp)
+    def _(step):
+        pl.semaphore_signal(barrier, inc=1, device_id={"tp": (my_tp + step) % tp})
+
+    pl.semaphore_wait(barrier, n + tp - 2)
 
     def k_copy(target, head):
         cols = pl.ds(pl.multiple_of(head * width, width), width)
@@ -77,6 +85,34 @@
             recv_sem=recv_o.at[me], device_id={"ep": source},
         )
 
+    def token_spot(owner):
+        return token_buf.at[pl.ds(pl.multiple_of(owner * tokens, tokens), tokens), :]
+
+    def token_copy(target):
+        return pltpu.make_async_remote_copy(
+            src_ref=token_ref, dst_ref=token_spot(my_tp), send_sem=send_t.at[target],
+            recv_sem=recv_t.at[my_tp], device_id={"tp": target},
+        )
+
+    def leave_copy(target):
+        return pltpu.make_async_remote_copy(
+            src_ref=leave_buf.at[target], dst_ref=routed_ref.at[me, my_tp],
+            send_sem=send_a.at[target], recv_sem=recv_a.at[me], device_id={"ep": target},
+        )
+
+    def spread_copy(source, target):
+        spot = routed_ref.at[source, my_tp]
+        return pltpu.make_async_remote_copy(
+            src_ref=spot, dst_ref=spot, send_sem=send_f.at[source, target],
+            recv_sem=recv_f.at[source, my_tp], device_id={"tp": target},
+        )
+
+    pltpu.make_async_copy(token_ref, token_spot(my_tp), recv_t.at[my_tp]).start()
+
+    @pl.loop(1, tp)
+    def _(step):
+        token_copy((my_tp + step) % tp).start()
+
     own_cols = pl.ds(pl.multiple_of(my_head * width, width), width)
     own_part = pl.ds(pl.multiple_of(my_member * chunk, chunk), chunk)
     pltpu.make_async_copy(k_ref.at[:, own_cols], k_buf.at[me], recv_k.at[me]).start()
@@ -92,6 +128,22 @@
     @pl.loop(1, n)
     def _(step):
         q_copy((me + step) % n).start()
+
+    @pl.loop(0, tp)
+    def _(owner):
+        pltpu.make_async_copy(token_spot(owner), token_spot(owner), recv_t.at[owner]).wait()
+
+    @pl.loop(0, n)
+    def _(target):
+        leave_buf[target] = jnp.dot(
+            pick_ref[target], token_buf[...], preferred_element_type=jnp.float32
+        ).astype(leave_buf.dtype)
+
+    pltpu.make_async_copy(leave_buf.at[me], routed_ref.at[me, my_tp], recv_a.at[me]).start()
+
+    @pl.loop(1, n)
+    def _(step):
+        leave_copy((me + step) % n).start()
 
     def landed(source):
         pltpu.make_async_copy(k_buf.at[source], k_buf.at[source], recv_k.at[source]).wait()
@@ -157,6 +209,14 @@
         def _():
             back_copy(i).start()
 
+        source = (me + n - i) % n
+        spot = routed_ref.at[source, my_tp]
+        pltpu.make_async_copy(spot, spot, recv_a.at[source]).wait()
+
+        @pl.loop(1, tp)
+        def _(step):
+            spread_copy(source, (my_tp + step) % tp).start()
+
     own = pltpu.make_async_copy(o_buf.at[me], out_ref.at[own_part, own_cols], recv_o.at[me])
     own.start()
 
@@ -170,6 +230,20 @@
     def _(step):
         q_copy((me + step) % n).wait_send()
         back_copy((me + step) % n).wait_send()
+        leave_copy((me + step) % n).wait_send()
+
+    @pl.loop(1, tp)
+    def _(step):
+        token_copy((my_tp + step) % tp).wait_send()
+
+    @pl.loop(0, n)
+    def _(source):
+        @pl.loop(1, tp)
+        def _(step):
+            other = (my_tp + step) % tp
+            spread_copy(source, other).wait_send()
+            spot = routed_ref.at[source, other]
+            pltpu.make_async_copy(spot, spot, recv_f.at[source, other]).wait()
 
     @pl.loop(0, heads)
     def _(step):
@@ -188,8 +262,9 @@
         pltpu.make_async_copy(spot, spot, recv_o.at[i]).wait()
 
 
-def attention(queries, key_rows, values, forget_log):
-    n = lax.axis_size("ep")
+def attention(queries, key_rows, values, forget_log, picks, normed):
+    n, tp = lax.axis_size("ep"), lax.axis_size("tp")
+    share, depth = picks.shape[1], normed.shape[1]
     rows, heads = queries.shape[0], forget_log.shape[1]
     width = queries.shape[1] // heads
     members = n // heads
@@ -204,18 +279,24 @@
     dma = pltpu.SemaphoreType.DMA
     blocks = n * (n + 1) // 2
     return pl.pallas_call(
-        functools.partial(attention_kernel, n, heads),
-        out_shape=jax.ShapeDtypeStruct((rows, heads * width), jnp.bfloat16),
-        in_specs=[vmem] * 5,
-        out_specs=vmem,
+        functools.partial(attention_kernel, n, tp, heads),
+        out_shape=(
+            jax.ShapeDtypeStruct((rows, heads * width), jnp.bfloat16),
+            jax.ShapeDtypeStruct((n, tp, share, depth), jnp.bfloat16),
+        ),
+        in_specs=[vmem] * 7,
+        out_specs=(vmem, vmem),
         scratch_shapes=[
             pltpu.VMEM((n, rows, width), jnp.bfloat16),
             pltpu.VMEM((n, rows, width), jnp.bfloat16),
             pltpu.VMEM((n, chunk, width), jnp.bfloat16),
             pltpu.VMEM((n, chunk, width), jnp.bfloat16),
+            pltpu.VMEM((tp * normed.shape[0], depth), jnp.bfloat16),
+            pltpu.VMEM((n, share, depth), jnp.bfloat16),
             dma((n,)), dma((n,)), dma((n,)), dma((n,)),
             dma((heads,)), dma((heads,)), dma((n,)), dma((n,)),
             dma((n, members)), dma((n, members)),
+            dma((tp,)), dma((tp,)), dma((n,)), dma((n,)), dma((n, tp)), dma((n, tp)),
         ],
         compiler_params=pltpu.CompilerParams(
             collective_id=0, has_side_effects=True, vmem_limit_bytes=40 * 1024 * 1024
@@ -224,7 +305,7 @@
             flops=40 * blocks * chunk * rows * width, bytes_accessed=8 * rows * heads * width,
             transcendentals=blocks * chunk * rows,
         ),
-    )(gate_row, gate_col, queries, key_rows, values)
+    )(gate_row, gate_col, queries, key_rows, values, picks, normed)
 
 
 def slot_places(route_rows, experts, capacity):
@@ -233,11 +314,6 @@
     earlier = jnp.cumsum(matches, axis=0) - matches
     ranking = jnp.sum(earlier * matches, axis=1)
     return entries * capacity + ranking
-
-
-def source_table(places, rows_count, chosen, total_slots):
-    owners = jnp.arange(places.shape[0], dtype=jnp.int32) // chosen
-    return jnp.full((total_slots,), rows_count, jnp.int32).at[places].set(owners)
 
 
 def body(
@@ -258,7 +334,6 @@
     center = jnp.mean(as_float, axis=1, keepdims=True)
     variance = jnp.mean(jnp.square(as_float - center), axis=1, keepdims=True)
     normed = ((as_float - center) * lax.rsqrt(variance + EPSILON) * norm_gain).astype(jnp.bfloat16)
-    group_rows = lax.all_gather(normed, "tp", axis=0, tiled=True)
     block_rows = route_ids.shape[0]
     chosen = route_ids.shape[1]
     expert_local = gate_weight.shape[0]
@@ -267,19 +342,20 @@
     experts = expert_local * ep_count
     capacity = block_rows * chosen * 2 // experts
     places = slot_places(route_ids, experts, capacity)
-    slot_table = source_table(places, block_rows, chosen, experts * capacity).reshape(
-        ep_count, expert_local, capacity
-    )
     share_size = capacity // tp_count
-    part_table = lax.dynamic_slice_in_dim(
-        slot_table, lax.axis_index("tp") * share_size, share_size, 2
-    )
-    outgoing = jnp.take(group_rows, part_table, axis=0, mode="fill", fill_value=0)
-    arrived = lax.all_to_all(outgoing, "ep", split_axis=0, concat_axis=0, tiled=True)
-    arrived, queries = lax.optimization_barrier((arrived, queries))
-    attended = attention(queries, key_rows, values, forget_log)
-    arrived_rows = lax.all_gather(arrived, "tp", axis=2, tiled=True)
-    arrived_rows, attended = lax.optimization_barrier((arrived_rows, attended))
+    own_slots = lax.axis_index("tp") * share_size + jnp.arange(share_size, dtype=jnp.int32)
+    part_slots = jnp.arange(experts, dtype=jnp.int32)[:, None] * capacity + own_slots[None, :]
+    picks = jnp.any(
+        part_slots.reshape(ep_count, expert_local * share_size)[:, :, None, None]
+        == places.reshape(block_rows, chosen).T[None, None, :, :],
+        axis=2,
+    ).astype(jnp.bfloat16)
+    attended, routed = attention(queries, key_rows, values, forget_log, picks, normed)
+    arrived_rows = (
+        routed.reshape(ep_count, tp_count, expert_local, share_size, routed.shape[3])
+        .transpose(0, 2, 1, 3, 4)
+        .reshape(ep_count, expert_local, capacity, routed.shape[3])
+    )
     gate_part = jnp.einsum(
         "sxcd,xdf->sxcf", arrived_rows, gate_weight, preferred_element_type=jnp.float32
     )

time: 225 us -> 215 us (0.956)
  blocking collectives: 31.7 us -> 0 us
  Pallas kernels: 59.9 us -> 89.8 us
  matrix products: 21.4 us -> 17.8 us
  waiting for transfers between devices: 73.2 us -> 70.7 us
    all_to_all x1 -> x0, blocking collectives: 31.7 us -> none  [body(): lax.all_to_all(outgoing, 'ep', split_axis=0, concat_axis=0, tiled=True)]
    pallas_call x1, Pallas kernels: 59.9 us -> 89.8 us  [attention(): pl.pallas_call(functools.partial(attention_kernel, n, tp, heads), out_sha...]
    all_gather x2 -> x0, waiting for transfers between devices: 14.9 us -> none  [the longest x1 14.9 us: body(): group_rows = lax.all_gather(normed, 'tp', axis=0, tiled=True)]
    all_gather x1, waiting for transfers between devices: 38.2 us -> 50.5 us  [body(): part_rows = lax.all_gather(flat_hidden, 'tp', axis=1, tiled=True)]
    dot_general x1, matrix products: 5.93 us -> 2.32 us  [body(): jnp.einsum('sxcd,xdf->sxcf', arrived_rows, gate_weight, preferred_element...]
    gather x1 -> x0, local copies, waits for them, and re-layouts: 3.56 us -> none  [body(): jnp.take(group_rows, part_table, axis=0, mode='fill', fill_value=0)]
    unnamed x16, local copies, waits for them, and re-layouts: 0.94 us -> 4.04 us
  transfers between devices with their start and end apart: 5 -> 3, of which waited for: 4 -> 3; matrix products, arithmetic and copies ran while one was open for 9% -> 6% of each run, Pallas kernels for 27% -> 0%
where the time goes in v2:
time: 215 us; the launch traced here: 214 us
  Pallas kernels  89.8 us (42%)
  waiting for transfers between devices  70.7 us (33%)
  matrix products  17.8 us (8%)
  between operations  14.3 us (7%)
  other arithmetic  8.92 us (4%)
  local copies, waits for them, and re-layouts  7.37 us (3%)
  starting transfers between devices  5.59 us (3%)
    pallas_call x1, Pallas kernels, attention(): pl.pallas_call(functools.partial(attention_kernel, n, tp, heads), out_sha...  89.8 us
    all_gather x1, waiting for transfers between devices, body(): part_rows = lax.all_gather(flat_hidden, 'tp', axis=1, tiled=True)  50.5 us
    all_gather x1, waiting for transfers between devices, body(): lax.all_gather(attended, 'tp', axis=1, tiled=True)  11.9 us
    all_to_all x1, waiting for transfers between devices, body(): lax.all_to_all(leaving, 'ep', split_axis=0, concat_axis=0, tiled=True)  7.55 us
    dot_general x1, matrix products, body(): jnp.einsum('sxcf,xfd->sxcd', shaped, down_weight, preferred_element_type=...  6.15 us
    dot_general x1, matrix products, body(): jnp.dot(lax.all_gather(attended, 'tp', axis=1, tiled=True), out_weight, p...  6.12 us
    all_to_all x1, starting transfers between devices, body(): lax.all_to_all(leaving, 'ep', split_axis=0, concat_axis=0, tiled=True)  5.51 us
  transfers between devices with their start and end apart: 3, of which 3 were waited for; matrix products, arithmetic and copies ran while one was open for 6% of the time, Pallas kernels for 0%

profile of v2, /device:TPU:0, one launch (start us, length us, event | category | flops | bytes accessed | tf_op | source)
XLA Modules:
  0.0 214.4 jit_solution(14300768749676686987)
XLA Ops:
  7.2 0.8 copy.36
  8.0 0.1 eq.45
  8.2 0.1 eq.41
  8.3 0.5 broadcast.137
  8.8 1.5 fusion.32
  10.4 0.3 reshape.188.gate_col
  10.8 0.6 reduce-window.6
  11.4 0.2 slice_reduce_fusion
  11.7 0.1 reduce_sum.41
  11.9 0.7 broadcast_multiply_fusion
  12.8 1.1 convert_reduce_fusion
  13.9 1.2 fusion.26
  15.1 1.1 fusion.28.token_ref
  16.3 1.0 copy-done
  17.3 1.0 copy-done.1
  18.3 1.0 copy-done.2
  19.4 89.8 %shard_map.131 = (bf16[512,512]{1,0:T(8,128)(2,1)}, bf16[8,4,16,4096]{3,2,1,0:T(8,128)(2,1)S(1)}) custom-call(f32[8,1,512]{2,1,0:T(1,128)S(1)} %bitcast.71, f32[8,256,1]{2,1,0:T(8,128)S(1)} %reshape.188.gate_col, bf16[512,512]{1,0:T(8,128)(2,1)S(1)} %copy-done, bf16[512,512]{1,0:T(8,128)(2,1)S(1)} %copy-done.1, bf16[512,512]{1,0:T(8,128)(2,1)S(1)} %copy-done.2, ...), custom_call_target="tpu_custom_call" | custom-call | flops 24159191040 | bytes 2097152 | tf_op jit(solution)/shard_map/pallas_call | solution.py:281
  109.2 2.3 %fusion.12 = f32[8,1,64,512]{3,2,0,1:T(8,128)S(1)} fusion(bf16[8,64,4096]{2,1,0:T(8,128)(2,1)S(1)} %bitcast.72, bf16[1,4096,512]{2,1,0:T(8,128)(2,1)S(1)} %copy-done.5), kind=kOutput, calls=%fused_computation.10 | convolution fusion | flops 2147483648 | bytes 9437184 | tf_op jit(solution)/shard_map/sxcd,xdf->sxcf/dot_general | solution.py:359
  111.5 3.2 %fusion.21 = bf16[8,1,64,512]{3,2,0,1:T(8,128)(2,1)} fusion(bf16[8,64,4096]{2,1,0:T(8,128)(2,1)S(1)} %bitcast.73, bf16[1,4096,512]{2,1,0:T(8,128)(2,1)S(1)} %copy-done.6, f32[8,1,64,512]{3,2,0,1:T(8,128)S(1)} %fusion.12), kind=kOutput, calls=%fused_computation.13 | convolution fusion | flops 2149056512 | bytes 9961472 | tf_op jit(solution)/shard_map/sxcd,xdf->sxcf/dot_general | solution.py:362
  114.8 0.7 all-gather.3.cloned.1.call-update
  115.5 50.5 %all-gather.5.cloned.1.call-done = bf16[512,2048]{1,0:T(8,128)(2,1)} async-done(((bf16[512,512]{1,0:T(8,128)(2,1)}), bf16[512,2048]{1,0:T(8,128)(2,1)}) %all-gather.5.cloned.1.call-update) | async-done | bytes 2097168 | tf_op jit(solution)/shard_map/all_gather | solution.py:374
  166.0 6.2 %fusion.9 = bf16[8,1,64,1024]{3,2,1,0:T(8,128)(2,1)} fusion(bf16[8,64,2048]{2,1,0:T(8,128)(2,1)} %bitcast.78, bf16[1,2048,1024]{2,1,0:T(8,128)(2,1)} %param.23), kind=kOutput, calls=%fused_computation.9 | convolution fusion | flops 2148007936 | bytes 7340032 | tf_op jit(solution)/shard_map/sxcf,xfd->sxcd/dot_general | solution.py:376
  172.2 5.5 %all-to-all-start = ((bf16[8,1,64,1024]{3,2,1,0:T(8,128)(2,1)}), bf16[8,1,64,1024]{3,2,1,0:T(8,128)(2,1)S(1)}, u32[]{:S(2)}, u32[]{:S(2)}) async-start(bf16[8,1,64,1024]{3,2,1,0:T(8,128)(2,1)} %fusion.9), calls=%async_computation | async-start | bytes 2097152 | tf_op jit(solution)/shard_map/all_to_all | solution.py:379
  177.8 0.1 mul.86
  178.0 0.1 copy.40
  178.1 0.1 copy.43
  178.2 11.9 %all-gather.3.cloned.1.call-done = bf16[512,2048]{1,0:T(8,128)(2,1)} async-done(((bf16[512,512]{1,0:T(8,128)(2,1)}), bf16[512,2048]{1,0:T(8,128)(2,1)}) %all-gather.3.cloned.1.call-update) | async-done | bytes 2097168 | tf_op jit(solution)/shard_map/all_gather | solution.py:370
  190.2 6.1 %convolution_convert_fusion = bf16[512,1024]{1,0:T(8,128)(2,1)} fusion(bf16[512,2048]{1,0:T(8,128)(2,1)} %all-gather.3.cloned.1.call-done, bf16[2048,1024]{1,0:T(8,128)(2,1)} %param.16), kind=kOutput, calls=%fused_computation.8 | convolution fusion | flops 2148007936 | bytes 7340032 | tf_op jit(solution)/shard_map/dot_general | solution.py:369
  196.3 7.5 %all-to-all-done = bf16[8,1,64,1024]{3,2,1,0:T(8,128)(2,1)S(1)} async-done(((bf16[8,1,64,1024]{3,2,1,0:T(8,128)(2,1)}), bf16[8,1,64,1024]{3,2,1,0:T(8,128)(2,1)S(1)}, u32[]{:S(2)}, u32[]{:S(2)}) %all-to-all-start) | async-done | bytes 1048608 | tf_op jit(solution)/shard_map/all_to_all | solution.py:379
  203.8 1.2 gather_fusion
  205.0 0.2 gather.7
  205.2 2.3 %multiply_reduce_fusion = bf16[128,1024]{1,0:T(8,128)(2,1)} fusion(bf16[128,2,1024]{2,1,0:T(2,128)(2,1)S(1)} %gather.7, pred[128,2]{1,0:T(8,128)(4,1)S(1)} %copy.40, f32[128,2]{1,0:T(8,128)S(1)} %copy.43), kind=kLoop, calls=%fused_computation.14 | loop fusion | flops 917504 | bytes 787712 | tf_op jit(solution)/shard_map/reduce_sum | solution.py:383
  (32 shorter events, 0.7 us)
Async XLA Ops:
  7.2 158.8 %all-gather.5.cloned.1.call-start = ((), (), s32[]{:S(2)}) async-start(), calls=%async_computation.2 | async-start | bytes 2621440 | tf_op jit(solution)/shard_map/all_gather | solution.py:374
  16.3 1.0 copy-start
  17.3 1.0 copy-start.1
  18.3 1.0 copy-start.2
  19.4 89.8 %copy-start.5 = (bf16[1,4096,512]{2,1,0:T(8,128)(2,1)S(1)}, bf16[1,4096,512]{2,1,0:T(8,128)(2,1)}, u32[]{:S(2)}) copy-start(bf16[1,4096,512]{2,1,0:T(8,128)(2,1)} %param.21) | copy-start | bytes 12582916
  109.2 2.3 %copy-start.6 = (bf16[1,4096,512]{2,1,0:T(8,128)(2,1)S(1)}, bf16[1,4096,512]{2,1,0:T(8,128)(2,1)}, u32[]{:S(2)}) copy-start(bf16[1,4096,512]{2,1,0:T(8,128)(2,1)} %param.22) | copy-start | bytes 12582916
  114.7 75.4 %all-gather.3.cloned.1.call-start = ((), (), s32[]{:S(2)}) async-start(), calls=%async_computation.1 | async-start | bytes 2621440 | tf_op jit(solution)/shard_map/all_gather | solution.py:370
  166.0 11.9 %copy-start.3 = (s32[128,2]{0,1:T(2,128)S(1)}, s32[128,2]{0,1:T(2,128)}, u32[]{:S(2)}) copy-start(s32[128,2]{0,1:T(2,128)} %param.19) | copy-start | bytes 3076
  166.0 12.1 %copy-start.4 = (f32[128,2]{0,1:T(2,128)S(1)}, f32[128,2]{0,1:T(2,128)}, u32[]{:S(2)}) copy-start(f32[128,2]{0,1:T(2,128)} %param.20) | copy-start | bytes 3076
  172.2 31.7 %all-to-all-start = ((bf16[8,1,64,1024]{3,2,1,0:T(8,128)(2,1)}), bf16[8,1,64,1024]{3,2,1,0:T(8,128)(2,1)S(1)}, u32[]{:S(2)}, u32[]{:S(2)}) async-start(bf16[8,1,64,1024]{3,2,1,0:T(8,128)(2,1)} %fusion.9), calls=%async_computation | async-start | bytes 2097152 | tf_op jit(solution)/shard_map/all_to_all | solution.py:379
Sparse Core Ops, SparseCore 0:
  114.8 51.1 all-gather.4
  167.6 22.5 all-gather.2
